TPU v7x, 32 devices: a whole 2x2x4 slice. The times are simulated.
32 devices in a mesh: fs: 8 (over z, y), tp: 4 (over x, core).
Axes of the slice: x: 2, y: 2, z: 4, core: 2. Of those that a mesh axis runs over, the one named last changes fastest.
Arguments:
- tokens: bfloat16 [8192, 2048], P('fs'), may hold values from -6 to 6
- norm_gain: float32 [2048], P('fs'), may hold values from 0.1 to 1.9
- gate_train: float32 [8, 2048, 768], P(None, 'fs', 'tp'), may hold values from -0.125 to 0.125
- up_train: float32 [8, 2048, 768], P(None, 'fs', 'tp'), may hold values from -0.125 to 0.125
- down_train: float32 [8, 768, 2048], P(None, 'fs', 'tp'), may hold values from -0.21875 to 0.21875
- expert_ids: int32 [8192, 2], P('fs'), may hold values from 0 to 7, all different within a row; in each aligned block of 1024 rows (0 to 1023, 1024 to 2047, ...) at most 512 rows name the same one
- route_weights: float32 [8192, 2], P('fs'), may hold values from 0.1 to 1
Outputs:
- gate_serve: bfloat16 [8, 2048, 768], P('fs', None, 'tp')
- up_serve: bfloat16 [8, 2048, 768], P('fs', None, 'tp')
- down_serve: bfloat16 [8, 768, 2048], P('fs', 'tp')
- mixed: bfloat16 [8192, 2048], P('fs', 'tp')
Inputs may be any that keep to these rules, and one draw needn't show every extreme that they name: `expert_ids`: each row names 2 different experts. Within each aligned block of 1024 rows no expert is named more than 512 times, and in every block some expert is named exactly 512 times; every expert is named somewhere.
All inputs are finite; a program needn't handle non-finite values.
Results may differ from a plain program's by a relative error of at most 0.011.
Values may be sent and summed in bfloat16 or wider, within the bound.
No kernel may reach another device: no remote copies, remote signals or barrier semaphores. Data moves between devices by JAX's collectives and lax.ppermute only.
A program may use at most 128 MiB of HBM per device.

v0:
```python
import jax
import jax.numpy as jnp
from jax import lax
from jax.sharding import PartitionSpec as P

epsilon = 1e-06


def on_device(tokens, norm_gain, gate_train, up_train, down_train, expert_ids, route_weights):
    fs_count = lax.axis_size("fs")
    tp_count = lax.axis_size("tp")
    experts = gate_train.shape[0]
    local_experts = experts // fs_count
    gate_cast = (norm_gain[None, :, None] * gate_train).astype(jnp.bfloat16)
    up_cast = (norm_gain[None, :, None] * up_train).astype(jnp.bfloat16)
    gate_serve, up_serve = (
        lax.all_to_all(gate_cast, "fs", split_axis=0, concat_axis=1, tiled=True),
        lax.all_to_all(up_cast, "fs", split_axis=0, concat_axis=1, tiled=True),
    )
    down_serve = lax.all_to_all(
        lax.all_to_all(
            down_train.astype(jnp.bfloat16), "fs", split_axis=0, concat_axis=1, tiled=True
        ),
        "tp",
        split_axis=1,
        concat_axis=2,
        tiled=True,
    )
    tok_float = tokens.astype(jnp.float32)
    normed = (
        tok_float * lax.rsqrt(jnp.mean(tok_float * tok_float, axis=-1, keepdims=True) + epsilon)
    ).astype(jnp.bfloat16)
    tok_rows, picks = expert_ids.shape
    width = tokens.shape[1]
    capacity = 2 * tok_rows * picks // experts
    flat_ids = expert_ids.reshape(-1)
    onehot = (flat_ids[:, None] == jnp.arange(experts, dtype=jnp.int32)[None, :]).astype(jnp.int32)
    slot_rank = jnp.sum((jnp.cumsum(onehot, axis=0) - onehot) * onehot, axis=1)
    target = (flat_ids * capacity + slot_rank).reshape(tok_rows, picks)
    slot_ids = jnp.arange(experts * capacity, dtype=jnp.int32)
    dispatch = jnp.zeros((experts * capacity, tok_rows), jnp.bfloat16)
    for pick in range(picks):
        dispatch = dispatch + (slot_ids[:, None] == target[None, :, pick]).astype(jnp.bfloat16)
    outgoing = jnp.dot(dispatch, normed, preferred_element_type=jnp.float32).astype(jnp.bfloat16)
    outgoing = outgoing.reshape(experts, capacity, width)
    quarter = capacity // tp_count
    gate_whole, up_whole, down_whole = (
        lax.all_gather(gate_serve, "tp", axis=2, tiled=True),
        lax.all_gather(up_serve, "tp", axis=2, tiled=True),
        lax.all_gather(down_serve, "tp", axis=1, tiled=True),
    )
    share_rows = lax.dynamic_slice_in_dim(outgoing, lax.axis_index("tp") * quarter, quarter, 1)
    routed = lax.all_to_all(share_rows, "fs", split_axis=0, concat_axis=1, tiled=True)
    gate_act = jnp.einsum("erd,edf->erf", routed, gate_whole, preferred_element_type=jnp.float32)
    up_act = jnp.einsum("erd,edf->erf", routed, up_whole, preferred_element_type=jnp.float32)
    hidden = (jax.nn.silu(gate_act) * up_act).astype(jnp.bfloat16)
    row_count = hidden.shape[1]
    block_width = hidden.shape[2] // tp_count
    hidden_blocks = hidden.reshape(local_experts, row_count, tp_count, block_width)
    down_blocks = down_whole.reshape(local_experts, tp_count, block_width, width)
    partial_value = jnp.einsum(
        "erbf,ebfd->erbd", hidden_blocks, down_blocks, preferred_element_type=jnp.float32
    )
    results = jnp.sum(partial_value.astype(jnp.bfloat16).astype(jnp.float32), axis=2).astype(
        jnp.bfloat16
    )
    returned = lax.all_to_all(
        lax.all_to_all(results, "fs", split_axis=1, concat_axis=0, tiled=True),
        "tp",
        split_axis=2,
        concat_axis=1,
        tiled=True,
    )
    returned_flat = returned.reshape(experts * capacity, returned.shape[2])
    shares = route_weights / jnp.sum(route_weights, axis=-1, keepdims=True)
    mixed = jnp.zeros((tok_rows, returned_flat.shape[1]), jnp.float32)
    for pick in range(picks):
        selector = (target[:, pick][:, None] == slot_ids[None, :]).astype(jnp.bfloat16)
        picked = jnp.dot(selector, returned_flat, preferred_element_type=jnp.float32)
        mixed = mixed + shares[:, pick][:, None] * picked
    return (gate_serve, up_serve, down_serve, mixed.astype(jnp.bfloat16))


def solution(mesh):
    return jax.shard_map(
        on_device,
        mesh=mesh,
        in_specs=(
            P("fs", None),
            P("fs"),
            P(None, "fs", "tp"),
            P(None, "fs", "tp"),
            P(None, "fs", "tp"),
            P("fs", None),
            P("fs", None),
        ),
        out_specs=(P("fs", None, "tp"), P("fs", None, "tp"), P("fs", "tp", None), P("fs", "tp")),
        check_vma=False,
    )
```

profile of v0, /device:TPU:0, one launch (start us, length us, event | category | flops | bytes accessed | tf_op | source)
XLA Modules:
  0.0 500.3 jit_solution(15567781841299172667)
XLA Ops:
  7.2 3.5 multiply_convert_fusion.1
  10.7 7.3 %all-to-all-start.1 = ((bf16[8,256,192]{1,2,0:T(8,128)(2,1)}), bf16[8,256,192]{1,2,0:T(8,128)(2,1)S(1)}, u32[]{:S(2)}, u32[]{:S(2)}) async-start(bf16[8,256,192]{1,2,0:T(8,128)(2,1)} %get-tuple-element.8), calls=%async_computation.1 | async-start | bytes 1572864 | tf_op jit(solution)/shard_map/all_to_all | solution.py:18
  18.0 1.0 convert_element_type.50
  19.0 19.2 %all-to-all-done.1 = bf16[8,256,192]{1,2,0:T(8,128)(2,1)S(1)} async-done(((bf16[8,256,192]{1,2,0:T(8,128)(2,1)}), bf16[8,256,192]{1,2,0:T(8,128)(2,1)S(1)}, u32[]{:S(2)}, u32[]{:S(2)}) %all-to-all-start.1) | async-done | bytes 786464 | tf_op jit(solution)/shard_map/all_to_all | solution.py:18
  38.1 3.6 all-to-all-start.2
  41.7 0.2 copy.62
  41.9 0.3 eq.85
  42.2 0.3 eq.81
  42.5 2.3 reduce-window.6
  44.8 0.3 slice_reduce_fusion
  45.2 16.9 %all-to-all-done.2 = bf16[8,96,512]{2,1,0:T(8,128)(2,1)S(1)} async-done(((bf16[8,96,512]{2,1,0:T(8,128)(2,1)}), bf16[8,96,512]{2,1,0:T(8,128)(2,1)S(1)}, u32[]{:S(2)}, u32[]{:S(2)}) %all-to-all-start.2) | async-done | bytes 786464 | tf_op jit(solution)/shard_map/all_to_all | solution.py:21
  62.1 3.5 all-to-all-start
  65.8 3.1 fusion.4
  68.9 0.4 copy.59
  69.3 1.2 all_to_all.70
  70.6 0.5 reduce_sum.45
  71.1 0.2 copy.64
  71.3 2.3 copy.78
  73.7 0.5 broadcast.37
  74.2 5.4 %reduce.7 = bf16[768,512]{1,0:T(8,128)(2,1)S(1)} reduce(bf16[768,1,512]{2,1,0:T(2,128)(2,1)S(1)} %bitcast.68, bf16[]{:T(256)} %broadcast.37), dimensions={1}, to_apply=%bitcast.63.reduce_sub_computation | reduce | bytes 1572866
  79.6 1.4 reshape.106
  81.0 5.0 %all-to-all-done = bf16[8,256,192]{1,2,0:T(8,128)(2,1)S(1)} async-done(((bf16[8,256,192]{1,2,0:T(8,128)(2,1)}), bf16[8,256,192]{1,2,0:T(8,128)(2,1)S(1)}, u32[]{:S(2)}, u32[]{:S(2)}) %all-to-all-start) | async-done | bytes 786464 | tf_op jit(solution)/shard_map/all_to_all | solution.py:17
  86.0 3.5 all-to-all-start.3
  89.5 11.2 %all-gather.4.cloned.1.call-start = ((), (), s32[]{:S(2)}) async-start(), calls=%async_computation.7 | async-start | bytes 3932160 | tf_op jit(solution)/shard_map/all_gather | solution.py:48
  100.8 23.5 %convolution_convert_fusion = bf16[4096,2048]{1,0:T(8,128)(2,1)} fusion(s32[1024]{0:T(1024)S(1)} %bitcast.79, s32[1024]{0:T(1024)S(1)} %bitcast.81, bf16[1024,2048]{1,0:T(8,128)(2,1)} %param.7, f32[1024]{0:T(1024)S(1)} %add_rsqrt_fusion), kind=kOutput, calls=%fused_computation.9 | convolution fusion | flops 17228103680 | bytes 20983808 | tf_op jit(solution)/shard_map/dot_general | solution.py:44
  124.3 0.4 copy.58
  124.7 1.2 all_to_all.33
  126.0 4.7 constant_dynamic-slice_fusion
  130.7 4.6 all-to-all-start.4
  135.4 0.8 reshape.107
  136.2 0.2 copy.70
  136.4 1.0 copy.72
  137.4 91.7 %all-to-all-done.4 = bf16[8,128,2048]{2,1,0:T(8,128)(2,1)} async-done(((bf16[8,128,2048]{2,1,0:T(8,128)(2,1)}), bf16[8,128,2048]{2,1,0:T(8,128)(2,1)}, u32[]{:S(2)}, u32[]{:S(2)}) %all-to-all-start.4) | async-done | bytes 4194336 | tf_op jit(solution)/shard_map/all_to_all | solution.py:53
  229.1 8.3 %fusion.15 = f32[1024,768]{0,1:T(8,128)} fusion(bf16[1024,2048]{1,0:T(8,128)(2,1)} %bitcast.7, bf16[1,2048,768]{1,2,0:T(8,128)(2,1)} %all-gather.6.cloned.1.call-done), kind=kOutput, calls=%fused_computation.20 | convolution fusion | flops 3221225472 | bytes 10485760 | tf_op jit(solution)/shard_map/erd,edf->erf/dot_general | solution.py:55
  237.5 7.9 %multiply_convert_fusion = bf16[1024,768]{0,1:T(8,128)(2,1)S(1)} fusion(f32[1024,768]{0,1:T(8,128)} %fusion.15, bf16[1024,2048]{1,0:T(8,128)(2,1)} %bitcast.7, bf16[1,2048,768]{1,2,0:T(8,128)(2,1)} %all-gather.4.cloned.1.call-done), kind=kOutput, calls=%fused_computation.24 | convolution fusion | flops 3225944064 | bytes 12058624 | tf_op jit(solution)/shard_map/erd,edf->erf/dot_general | solution.py:54
  245.4 9.6 %convert_reduce_fusion = bf16[1024,2048]{1,0:T(8,128)(2,1)} fusion(bf16[1024,4,192]{0,2,1:T(8,128)(2,1)S(1)} %bitcast.86, bf16[4,192,2048]{2,1,0:T(8,128)(2,1)} %bitcast.85), kind=kOutput, calls=%fused_computation.1 | convolution fusion | flops 3235905536 | bytes 8912896 | tf_op jit(solution)/shard_map/erbf,ebfd->erbd/dot_general | solution.py:61
  255.0 8.6 %copy.77 = bf16[1,1024,2048]{2,0,1:T(2,128)(2,1)} copy(bf16[1,1024,2048]{2,1,0:T(8,128)(2,1)} %bitcast.70) | data formatting | bytes 8388608 | tf_op jit(solution)/shard_map/reduce_sum | solution.py:64
  263.6 26.9 %reduce.8 = bf16[1024,2048]{1,0:T(8,128)(2,1)} reduce(bf16[1024,1,2048]{2,1,0:T(2,128)(2,1)} %bitcast.65, bf16[]{:T(256)} %broadcast.37), dimensions={1}, to_apply=%bitcast.62.reduce_sub_computation | reduce | bytes 8388610
  290.5 7.8 %reshape.108 = bf16[8,2,131072]{2,1,0:T(2,128)(2,1)} reshape(bf16[1024,2048]{1,0:T(8,128)(2,1)} %reduce.8) | data formatting | bytes 8388608
  298.3 97.7 %all_to_all.90 = bf16[8,2,131072]{2,1,0:T(2,128)(2,1)} all-to-all(bf16[8,2,131072]{2,1,0:T(2,128)(2,1)} %reshape.108), channel_id=1, replica_groups=mesh['fs'=8,'tp'=4] {'fs'}, dimensions={0} | all-to-all | bytes 8388608 | tf_op jit(solution)/shard_map/all_to_all | solution.py:68
  396.0 8.7 %reshape.109 = bf16[1024,1,2048]{2,1,0:T(2,128)(2,1)} reshape(bf16[8,2,131072]{2,1,0:T(2,128)(2,1)} %all_to_all.90) | data formatting | bytes 8388608
  404.7 8.0 %copy.71 = bf16[1,1024,2048]{2,1,0:T(8,128)(2,1)} copy(bf16[1,1024,2048]{2,0,1:T(2,128)(2,1)} %bitcast.66) | data formatting | bytes 8388608
  412.7 6.8 %copy.66 = bf16[8,128,2048]{1,0,2:T(8,128)(2,1)} copy(bf16[8,128,2048]{2,1,0:T(8,128)(2,1)} %bitcast.67) | data formatting | bytes 8388608 | tf_op jit(solution)/shard_map/all_to_all | solution.py:68
  419.5 5.0 all-to-all-start.6
  424.6 48.1 %all-to-all-done.6 = bf16[8,128,2048]{1,0,2:T(8,128)(2,1)} async-done(((bf16[8,128,2048]{1,0,2:T(8,128)(2,1)}), bf16[8,128,2048]{1,0,2:T(8,128)(2,1)}, u32[]{:S(2)}, u32[]{:S(2)}) %all-to-all-start.6) | async-done | bytes 4194336 | tf_op jit(solution)/shard_map/all_to_all | solution.py:67
  472.7 7.6 %copy.68 = bf16[8,4,128,512]{3,2,1,0:T(8,128)(2,1)} copy(bf16[8,4,128,512]{2,0,3,1:T(8,128)(2,1)} %bitcast.15) | data formatting | bytes 8388608 | tf_op jit(solution)/shard_map/all_to_all | solution.py:67
  480.3 7.5 %fusion = f32[1024,512]{1,0:T(8,128)S(1)} fusion(bf16[4096,512]{1,0:T(8,128)(2,1)} %bitcast.71, s32[1024]{0:T(1024)S(1)} %bitcast.82), kind=kOutput, calls=%fused_computation.5 | convolution fusion | flops 4299161600 | bytes 6295552 | tf_op jit(solution)/shard_map/dot_general | solution.py:79
  487.8 5.6 %add_convert_fusion = bf16[1024,512]{1,0:T(8,128)(2,1)} fusion(f32[1024,512]{1,0:T(8,128)S(1)} %fusion, bf16[4096,512]{1,0:T(8,128)(2,1)S(1)} %bitcast.72, s32[1024]{0:T(1024)S(1)} %bitcast.80, f32[1024]{0:T(1024)S(1)} %bitcast.84, f32[1024]{0:T(1024)S(1)} %bitcast.83), kind=kOutput, calls=%fused_computation.25 | convolution fusion | flops 4301258752 | bytes 7352320 | tf_op jit(solution)/shard_map/dot_general | solution.py:79
  (29 shorter events, 0.6 us)
Async XLA Ops:
  7.2 10.8 %copy-start.2 = (f32[8,96,512]{2,1,0:T(8,128)S(1)}, f32[8,96,512]{2,1,0:T(8,128)}, u32[]{:S(2)}) copy-start(f32[8,96,512]{2,1,0:T(8,128)} %param.11) | copy-start | bytes 4718596
  7.2 34.5 %copy-start.3 = (s32[1024,2]{0,1:T(2,128)S(1)}, s32[1024,2]{0,1:T(2,128)}, u32[]{:S(2)}) copy-start(s32[1024,2]{0,1:T(2,128)} %param.12) | copy-start | bytes 24580
  10.7 27.5 %all-to-all-start.1 = ((bf16[8,256,192]{1,2,0:T(8,128)(2,1)}), bf16[8,256,192]{1,2,0:T(8,128)(2,1)S(1)}, u32[]{:S(2)}, u32[]{:S(2)}) async-start(bf16[8,256,192]{1,2,0:T(8,128)(2,1)} %get-tuple-element.8), calls=%async_computation.1 | async-start | bytes 1572864 | tf_op jit(solution)/shard_map/all_to_all | solution.py:18
  38.1 24.0 %all-to-all-start.2 = ((bf16[8,96,512]{2,1,0:T(8,128)(2,1)}), bf16[8,96,512]{2,1,0:T(8,128)(2,1)S(1)}, u32[]{:S(2)}, u32[]{:S(2)}) async-start(bf16[8,96,512]{2,1,0:T(8,128)(2,1)} %convert_element_type.50), calls=%async_computation.2 | async-start | bytes 1572864 | tf_op jit(solution)/shard_map/all_to_all | solution.py:21
  62.1 3.7 copy-start.1
  62.1 23.9 %all-to-all-start = ((bf16[8,256,192]{1,2,0:T(8,128)(2,1)}), bf16[8,256,192]{1,2,0:T(8,128)(2,1)S(1)}, u32[]{:S(2)}, u32[]{:S(2)}) async-start(bf16[8,256,192]{1,2,0:T(8,128)(2,1)} %get-tuple-element.9), calls=%async_computation | async-start | bytes 1572864 | tf_op jit(solution)/shard_map/all_to_all | solution.py:17
  65.7 71.7 %all-gather.6.cloned.1.call-start = ((), (), s32[]{:S(2)}) async-start(), calls=%async_computation.8 | async-start | bytes 3932160 | tf_op jit(solution)/shard_map/all_gather | solution.py:49
  86.0 44.7 %all-to-all-start.3 = ((bf16[4,2,49152]{2,1,0:T(2,128)(2,1)}), bf16[4,2,49152]{2,1,0:T(2,128)(2,1)S(1)}, u32[]{:S(2)}, u32[]{:S(2)}) async-start(bf16[4,2,49152]{2,1,0:T(2,128)(2,1)} %reshape.106), calls=%async_computation.3 | async-start | bytes 1572864 | tf_op jit(solution)/shard_map/all_to_all | solution.py:20
  89.5 147.9 %all-gather.4.cloned.1.call-start = ((), (), s32[]{:S(2)}) async-start(), calls=%async_computation.7 | async-start | bytes 3932160 | tf_op jit(solution)/shard_map/all_gather | solution.py:48
  130.7 98.4 %all-to-all-start.4 = ((bf16[8,128,2048]{2,1,0:T(8,128)(2,1)}), bf16[8,128,2048]{2,1,0:T(8,128)(2,1)}, u32[]{:S(2)}, u32[]{:S(2)}) async-start(bf16[8,128,2048]{2,1,0:T(8,128)(2,1)} %constant_dynamic-slice_fusion), calls=%async_computation.4 | async-start | bytes 8388608 | tf_op jit(solution)/shard_map/all_to_all | solution.py:53
  135.3 110.0 %all-gather.8.cloned.1.call-start = ((), (), s32[]{:S(2)}) async-start(), calls=%async_computation.9 | async-start | bytes 3932160 | tf_op jit(solution)/shard_map/all_gather | solution.py:50
  419.5 5.0 copy-start.4
  419.5 53.2 %all-to-all-start.6 = ((bf16[8,128,2048]{1,0,2:T(8,128)(2,1)}), bf16[8,128,2048]{1,0,2:T(8,128)(2,1)}, u32[]{:S(2)}, u32[]{:S(2)}) async-start(bf16[8,128,2048]{1,0,2:T(8,128)(2,1)} %copy.66), calls=%async_computation.6 | async-start | bytes 8388608 | tf_op jit(solution)/shard_map/all_to_all | solution.py:67
  480.3 7.5 %copy-start = (bf16[8,4,128,512]{3,2,1,0:T(8,128)(2,1)S(1)}, bf16[8,4,128,512]{3,2,1,0:T(8,128)(2,1)}, u32[]{:S(2)}) copy-start(bf16[8,4,128,512]{3,2,1,0:T(8,128)(2,1)} %copy.68) | copy-start | bytes 12582916
Sparse Core Ops, SparseCore 0:
  70.7 36.2 all-gather.5
  126.1 27.6 all-gather.3
  156.0 28.4 all-gather.7
where the time goes:
time: 510 us; the launch traced here: 500 us
  waiting for transfers between devices  181 us (35%)
  blocking collectives  97.7 us (19%)
  local copies, waits for them, and re-layouts  63.5 us (12%)
  matrix products  62.4 us (12%)
  other arithmetic  42.5 us (8%)
  starting transfers between devices  38.8 us (8%)
  between operations  14.4 us (3%)
    all_to_all x1, blocking collectives, on_device(): lax.all_to_all(results, 'fs', split_axis=1, concat_axis=0, tiled=True)  97.7 us
    all_to_all x1, waiting for transfers between devices, on_device(): lax.all_to_all(share_rows, 'fs', split_axis=0, concat_axis=1, tiled=True)  91.7 us
    all_to_all x1, waiting for transfers between devices, on_device(): lax.all_to_all(lax.all_to_all(results, 'fs', split_axis=1, concat_axis=0,...  48.1 us
    unnamed x3, other arithmetic  32.4 us
    unnamed x18, local copies, waits for them, and re-layouts  27.6 us
    dot_general x1, matrix products, on_device(): jnp.dot(dispatch, normed, preferred_element_type=jnp.float32)  23.5 us
    all_to_all x1, waiting for transfers between devices, on_device(): lax.all_to_all(up_cast, 'fs', split_axis=0, concat_axis=1, tiled=True)  19.2 us
    all_to_all x1, waiting for transfers between devices, on_device(): lax.all_to_all(down_train.astype(jnp.bfloat16), 'fs', split_axis=0, conca...  16.9 us
  transfers between devices with their start and end apart: 9, of which 5 were waited for; matrix products, arithmetic and copies ran while one was open for 13% of the time, Pallas kernels for 0%

commit v1 on v0

--- a/solution.py
+++ b/solution.py
@@ -65,7 +65,10 @@
         jnp.bfloat16
     )
     returned = lax.all_to_all(
-        lax.all_to_all(results, "fs", split_axis=1, concat_axis=0, tiled=True),
+        jnp.concatenate(
+            lax.all_to_all(jnp.stack(jnp.split(results, lax.axis_size("fs"), axis=1)), "fs", 0, 0),
+            axis=0,
+        ),
         "tp",
         split_axis=2,
         concat_axis=1,

time: 510 us -> 462 us (0.906)
  other arithmetic: 42.5 us -> 15.6 us
  starting transfers between devices: 38.8 us -> 28.3 us
  local copies, waits for them, and re-layouts: 63.5 us -> 54.3 us
    unnamed x3 -> x2, other arithmetic: 32.4 us -> 5.51 us
    unnamed x18 -> x24, local copies, waits for them, and re-layouts: 27.6 us -> 13.3 us
    reshape x0 -> x1, local copies, waits for them, and re-layouts: none -> 13.2 us  [on_device(): jnp.concatenate(lax.all_to_all(jnp.stack(jnp.split(results, lax.axis_size...]
    all_gather x1, starting transfers between devices: 11.2 us -> 0.51 us  [on_device(): lax.all_gather(gate_serve, 'tp', axis=2, tiled=True)]
    reduce_sum x1 -> x0, local copies, waits for them, and re-layouts: 8.63 us -> none  [on_device(): jnp.sum(partial_value.astype(jnp.bfloat16).astype(jnp.float32), axis=2)]
    another operation x0 -> x2, local copies, waits for them, and re-layouts: none -> 7.3 us  [on_device(): jnp.stack(jnp.split(results, lax.axis_size('fs'), axis=1))]
    all_to_all x2 -> x1, local copies, waits for them, and re-layouts: 14.4 us -> 7.53 us  [on_device(): lax.all_to_all(jnp.concatenate(lax.all_to_all(jnp.stack(jnp.split(results...]
  transfers between devices with their start and end apart: 9 -> 9, of which waited for: 5 -> 5; matrix products, arithmetic and copies ran while one was open for 13% -> 14% of each run, Pallas kernels for 0% -> 0%
where the time goes in v1:
time: 462 us; the launch traced here: 453 us
  waiting for transfers between devices  181 us (39%)
  blocking collectives  97.1 us (21%)
  matrix products  62.4 us (14%)
  local copies, waits for them, and re-layouts  54.3 us (12%)
  starting transfers between devices  28.3 us (6%)
  other arithmetic  15.6 us (3%)
  between operations  14.2 us (3%)
    all_to_all x1, blocking collectives, on_device(): lax.all_to_all(jnp.stack(jnp.split(results, lax.axis_size('fs'), axis=1))...  97.1 us
    all_to_all x1, waiting for transfers between devices, on_device(): lax.all_to_all(share_rows, 'fs', split_axis=0, concat_axis=1, tiled=True)  92 us
    all_to_all x1, waiting for transfers between devices, on_device(): lax.all_to_all(jnp.concatenate(lax.all_to_all(jnp.stack(jnp.split(results...  48.1 us
    dot_general x1, matrix products, on_device(): jnp.dot(dispatch, normed, preferred_element_type=jnp.float32)  23.5 us
    all_to_all x1, waiting for transfers between devices, on_device(): lax.all_to_all(up_cast, 'fs', split_axis=0, concat_axis=1, tiled=True)  19.2 us
    all_to_all x1, waiting for transfers between devices, on_device(): lax.all_to_all(down_train.astype(jnp.bfloat16), 'fs', split_axis=0, conca...  16.9 us
    unnamed x24, local copies, waits for them, and re-layouts  13.3 us
    reshape x1, local copies, waits for them, and re-layouts, on_device(): jnp.concatenate(lax.all_to_all(jnp.stack(jnp.split(results, lax.axis_size...  13.2 us
  transfers between devices with their start and end apart: 9, of which 5 were waited for; matrix products, arithmetic and copies ran while one was open for 14% of the time, Pallas kernels for 0%

profile of v1, /device:TPU:0, one launch (start us, length us, event | category | flops | bytes accessed | tf_op | source)
XLA Modules:
  0.0 453.2 jit_solution(702104543534435705)
XLA Ops:
  7.2 3.5 multiply_convert_fusion.1
  10.7 7.3 %all-to-all-start.1 = ((bf16[8,256,192]{1,2,0:T(8,128)(2,1)}), bf16[8,256,192]{1,2,0:T(8,128)(2,1)S(1)}, u32[]{:S(2)}, u32[]{:S(2)}) async-start(bf16[8,256,192]{1,2,0:T(8,128)(2,1)} %get-tuple-element.8), calls=%async_computation.1 | async-start | bytes 1572864 | tf_op jit(solution)/shard_map/all_to_all | solution.py:18
  18.0 1.0 convert_element_type.50
  19.0 19.2 %all-to-all-done.1 = bf16[8,256,192]{1,2,0:T(8,128)(2,1)S(1)} async-done(((bf16[8,256,192]{1,2,0:T(8,128)(2,1)}), bf16[8,256,192]{1,2,0:T(8,128)(2,1)S(1)}, u32[]{:S(2)}, u32[]{:S(2)}) %all-to-all-start.1) | async-done | bytes 786464 | tf_op jit(solution)/shard_map/all_to_all | solution.py:18
  38.1 3.6 all-to-all-start.2
  41.9 0.3 eq.85
  42.5 2.3 reduce-window.6
  44.8 0.3 slice_reduce_fusion
  45.2 16.9 %all-to-all-done.2 = bf16[8,96,512]{2,1,0:T(8,128)(2,1)S(1)} async-done(((bf16[8,96,512]{2,1,0:T(8,128)(2,1)}), bf16[8,96,512]{2,1,0:T(8,128)(2,1)S(1)}, u32[]{:S(2)}, u32[]{:S(2)}) %all-to-all-start.2) | async-done | bytes 786464 | tf_op jit(solution)/shard_map/all_to_all | solution.py:21
  62.1 3.5 all-to-all-start
  65.8 3.1 fusion.4
  68.9 0.4 copy.58
  69.3 1.2 all_to_all.64
  70.6 0.5 reduce_sum.45
  71.3 2.3 copy.74
  73.7 0.5 broadcast.37
  74.2 5.4 %reduce.7 = bf16[768,512]{1,0:T(8,128)(2,1)S(1)} reduce(bf16[768,1,512]{2,1,0:T(2,128)(2,1)S(1)} %bitcast.94, bf16[]{:T(256)} %broadcast.37), dimensions={1}, to_apply=%bitcast.91.reduce_sub_computation | reduce | bytes 1572866
  79.6 1.4 reshape.107
  81.0 5.0 %all-to-all-done = bf16[8,256,192]{1,2,0:T(8,128)(2,1)S(1)} async-done(((bf16[8,256,192]{1,2,0:T(8,128)(2,1)}), bf16[8,256,192]{1,2,0:T(8,128)(2,1)S(1)}, u32[]{:S(2)}, u32[]{:S(2)}) %all-to-all-start) | async-done | bytes 786464 | tf_op jit(solution)/shard_map/all_to_all | solution.py:17
  86.0 3.5 all-to-all-start.3
  89.5 0.5 all-gather.4.cloned.1.call-start
  90.0 23.5 %convolution_convert_fusion = bf16[4096,2048]{1,0:T(8,128)(2,1)} fusion(s32[1024]{0:T(1024)S(1)} %bitcast.112, s32[1024]{0:T(1024)S(1)} %bitcast.114, bf16[1024,2048]{1,0:T(8,128)(2,1)} %param.7, f32[1024]{0:T(1024)S(1)} %add_rsqrt_fusion), kind=kOutput, calls=%fused_computation.9 | convolution fusion | flops 17228103680 | bytes 20983808 | tf_op jit(solution)/shard_map/dot_general | solution.py:44
  113.6 0.4 copy.57
  114.0 1.2 all_to_all.62
  115.3 4.7 %constant_dynamic-slice_fusion = bf16[8,128,2048]{2,1,0:T(8,128)(2,1)} fusion(bf16[8,512,2048]{2,1,0:T(8,128)(2,1)} %bitcast.110, s32[]{:T(128)S(6)} %select_n.3), kind=kLoop, calls=%fused_computation.56 | loop fusion | bytes 8388612 | tf_op jit(solution)/shard_map/dynamic_slice | solution.py:52
  120.0 4.6 %all-to-all-start.4 = ((bf16[8,128,2048]{2,1,0:T(8,128)(2,1)}), bf16[8,128,2048]{2,1,0:T(8,128)(2,1)}, u32[]{:S(2)}, u32[]{:S(2)}) async-start(bf16[8,128,2048]{2,1,0:T(8,128)(2,1)} %constant_dynamic-slice_fusion), calls=%async_computation.4 | async-start | bytes 8388608 | tf_op jit(solution)/shard_map/all_to_all | solution.py:53
  124.6 0.8 reshape.108
  125.6 1.0 copy.70
  126.6 92.0 %all-to-all-done.4 = bf16[8,128,2048]{2,1,0:T(8,128)(2,1)} async-done(((bf16[8,128,2048]{2,1,0:T(8,128)(2,1)}), bf16[8,128,2048]{2,1,0:T(8,128)(2,1)}, u32[]{:S(2)}, u32[]{:S(2)}) %all-to-all-start.4) | async-done | bytes 4194336 | tf_op jit(solution)/shard_map/all_to_all | solution.py:53
  218.7 8.3 %fusion.15 = f32[1024,768]{0,1:T(8,128)} fusion(bf16[1024,2048]{1,0:T(8,128)(2,1)} %bitcast.7, bf16[1,2048,768]{1,2,0:T(8,128)(2,1)} %all-gather.6.cloned.1.call-done), kind=kOutput, calls=%fused_computation.20 | convolution fusion | flops 3221225472 | bytes 10485760 | tf_op jit(solution)/shard_map/erd,edf->erf/dot_general | solution.py:55
  227.0 7.9 %multiply_convert_fusion = bf16[1024,768]{0,1:T(8,128)(2,1)S(1)} fusion(f32[1024,768]{0,1:T(8,128)} %fusion.15, bf16[1024,2048]{1,0:T(8,128)(2,1)} %bitcast.7, bf16[1,2048,768]{1,2,0:T(8,128)(2,1)} %all-gather.4.cloned.1.call-done), kind=kOutput, calls=%fused_computation.24 | convolution fusion | flops 3225944064 | bytes 12058624 | tf_op jit(solution)/shard_map/erd,edf->erf/dot_general | solution.py:54
  234.9 9.6 %convert_reduce_fusion = bf16[1024,2048]{1,0:T(8,128)(2,1)} fusion(bf16[1024,4,192]{0,2,1:T(8,128)(2,1)S(1)} %bitcast.119, bf16[4,192,2048]{2,1,0:T(8,128)(2,1)} %bitcast.118), kind=kOutput, calls=%fused_computation.1 | convolution fusion | flops 3235905536 | bytes 8912896 | tf_op jit(solution)/shard_map/erbf,ebfd->erbd/dot_general | solution.py:61
  244.5 2.0 fusion.28
  246.6 1.9 fusion.27
  248.5 1.9 fusion.26
  250.3 1.9 fusion.25
  252.2 0.9 fusion.24
  253.1 0.8 fusion.23
  253.9 0.8 fusion.22
  254.8 0.9 fusion.21
  255.6 6.4 %copy.64 = bf16[8,1,128,2048]{2,3,1,0:T(8,128)(2,1)} copy(bf16[8,1,128,2048]{3,2,1,0:T(8,128)(2,1)} %fusion.21) | data formatting | bytes 8388608 | tf_op jit(solution)/shard_map/stack | solution.py:69
  262.0 97.1 %all_to_all.83 = bf16[8,1,128,2048]{2,3,1,0:T(8,128)(2,1)S(1)} all-to-all(bf16[8,1,128,2048]{2,3,1,0:T(8,128)(2,1)} %copy.64), channel_id=1, replica_groups=mesh['fs'=8,'tp'=4] {'fs'}, dimensions={0} | all-to-all | bytes 8388608 | tf_op jit(solution)/shard_map/all_to_all | solution.py:69
  359.2 13.2 %copy.65 = bf16[8,128,2048]{1,0,2:T(8,128)(2,1)} copy(bf16[8,128,2048]{1,2,0:T(8,128)(2,1)S(1)} %bitcast.93) | data formatting | bytes 8388608 | tf_op jit(solution)/shard_map/reshape | solution.py:68
  372.4 5.2 %all-to-all-start.6 = ((bf16[8,128,2048]{1,0,2:T(8,128)(2,1)}), bf16[8,128,2048]{1,0,2:T(8,128)(2,1)}, u32[]{:S(2)}, u32[]{:S(2)}) async-start(bf16[8,128,2048]{1,0,2:T(8,128)(2,1)} %copy.65), calls=%async_computation.6 | async-start | bytes 8388608 | tf_op jit(solution)/shard_map/all_to_all | solution.py:67
  377.7 48.1 %all-to-all-done.6 = bf16[8,128,2048]{1,0,2:T(8,128)(2,1)} async-done(((bf16[8,128,2048]{1,0,2:T(8,128)(2,1)}), bf16[8,128,2048]{1,0,2:T(8,128)(2,1)}, u32[]{:S(2)}, u32[]{:S(2)}) %all-to-all-start.6) | async-done | bytes 4194336 | tf_op jit(solution)/shard_map/all_to_all | solution.py:67
  425.8 7.5 %copy.67 = bf16[8,4,128,512]{3,2,1,0:T(8,128)(2,1)} copy(bf16[8,4,128,512]{2,0,3,1:T(8,128)(2,1)} %bitcast.24) | data formatting | bytes 8388608 | tf_op jit(solution)/shard_map/all_to_all | solution.py:67
  433.3 7.5 %fusion = f32[1024,512]{1,0:T(8,128)S(1)} fusion(bf16[4096,512]{1,0:T(8,128)(2,1)} %bitcast.104, s32[1024]{0:T(1024)S(1)} %bitcast.115), kind=kOutput, calls=%fused_computation.5 | convolution fusion | flops 4299161600 | bytes 6295552 | tf_op jit(solution)/shard_map/dot_general | solution.py:82
  440.8 5.6 %add_convert_fusion = bf16[1024,512]{1,0:T(8,128)(2,1)} fusion(f32[1024,512]{1,0:T(8,128)S(1)} %fusion, bf16[4096,512]{1,0:T(8,128)(2,1)S(1)} %bitcast.105, s32[1024]{0:T(1024)S(1)} %bitcast.113, f32[1024]{0:T(1024)S(1)} %bitcast.117, f32[1024]{0:T(1024)S(1)} %bitcast.116), kind=kOutput, calls=%fused_computation.25 | convolution fusion | flops 4301258752 | bytes 7352320 | tf_op jit(solution)/shard_map/dot_general | solution.py:82
  (35 shorter events, 1.4 us)
Async XLA Ops:
  7.2 10.8 %copy-start.3 = (f32[8,96,512]{2,1,0:T(8,128)S(1)}, f32[8,96,512]{2,1,0:T(8,128)}, u32[]{:S(2)}) copy-start(f32[8,96,512]{2,1,0:T(8,128)} %param.11) | copy-start | bytes 4718596
  7.2 34.5 %copy-start.4 = (s32[1024,2]{0,1:T(2,128)S(1)}, s32[1024,2]{0,1:T(2,128)}, u32[]{:S(2)}) copy-start(s32[1024,2]{0,1:T(2,128)} %param.12) | copy-start | bytes 24580
  10.7 27.5 %all-to-all-start.1 = ((bf16[8,256,192]{1,2,0:T(8,128)(2,1)}), bf16[8,256,192]{1,2,0:T(8,128)(2,1)S(1)}, u32[]{:S(2)}, u32[]{:S(2)}) async-start(bf16[8,256,192]{1,2,0:T(8,128)(2,1)} %get-tuple-element.8), calls=%async_computation.1 | async-start | bytes 1572864 | tf_op jit(solution)/shard_map/all_to_all | solution.py:18
  38.1 24.0 %all-to-all-start.2 = ((bf16[8,96,512]{2,1,0:T(8,128)(2,1)}), bf16[8,96,512]{2,1,0:T(8,128)(2,1)S(1)}, u32[]{:S(2)}, u32[]{:S(2)}) async-start(bf16[8,96,512]{2,1,0:T(8,128)(2,1)} %convert_element_type.50), calls=%async_computation.2 | async-start | bytes 1572864 | tf_op jit(solution)/shard_map/all_to_all | solution.py:21
  62.1 3.7 copy-start.2
  62.1 23.9 %all-to-all-start = ((bf16[8,256,192]{1,2,0:T(8,128)(2,1)}), bf16[8,256,192]{1,2,0:T(8,128)(2,1)S(1)}, u32[]{:S(2)}, u32[]{:S(2)}) async-start(bf16[8,256,192]{1,2,0:T(8,128)(2,1)} %get-tuple-element.9), calls=%async_computation | async-start | bytes 1572864 | tf_op jit(solution)/shard_map/all_to_all | solution.py:17
  65.7 61.0 %all-gather.6.cloned.1.call-start = ((), (), s32[]{:S(2)}) async-start(), calls=%async_computation.8 | async-start | bytes 3932160 | tf_op jit(solution)/shard_map/all_gather | solution.py:49
  86.0 34.0 %all-to-all-start.3 = ((bf16[4,2,49152]{2,1,0:T(2,128)(2,1)}), bf16[4,2,49152]{2,1,0:T(2,128)(2,1)S(1)}, u32[]{:S(2)}, u32[]{:S(2)}) async-start(bf16[4,2,49152]{2,1,0:T(2,128)(2,1)} %reshape.107), calls=%async_computation.3 | async-start | bytes 1572864 | tf_op jit(solution)/shard_map/all_to_all | solution.py:20
  89.5 137.5 %all-gather.4.cloned.1.call-start = ((), (), s32[]{:S(2)}) async-start(), calls=%async_computation.7 | async-start | bytes 3932160 | tf_op jit(solution)/shard_map/all_gather | solution.py:48
  120.0 98.7 %all-to-all-start.4 = ((bf16[8,128,2048]{2,1,0:T(8,128)(2,1)}), bf16[8,128,2048]{2,1,0:T(8,128)(2,1)}, u32[]{:S(2)}, u32[]{:S(2)}) async-start(bf16[8,128,2048]{2,1,0:T(8,128)(2,1)} %constant_dynamic-slice_fusion), calls=%async_computation.4 | async-start | bytes 8388608 | tf_op jit(solution)/shard_map/all_to_all | solution.py:53
  124.6 110.3 %all-gather.8.cloned.1.call-start = ((), (), s32[]{:S(2)}) async-start(), calls=%async_computation.9 | async-start | bytes 3932160 | tf_op jit(solution)/shard_map/all_gather | solution.py:50
  244.5 7.7 %copy-start = (bf16[1024,2048]{1,0:T(8,128)(2,1)S(1)}, bf16[1024,2048]{1,0:T(8,128)(2,1)}, u32[]{:S(2)}) copy-start(bf16[1024,2048]{1,0:T(8,128)(2,1)} %convert_reduce_fusion) | copy-start | bytes 12582916
  372.4 5.2 %copy-start.5 = (f32[1024,2]{0,1:T(2,128)S(1)}, f32[1024,2]{0,1:T(2,128)}, u32[]{:S(2)}) copy-start(f32[1024,2]{0,1:T(2,128)} %param.13) | copy-start | bytes 24580
  372.4 53.4 %all-to-all-start.6 = ((bf16[8,128,2048]{1,0,2:T(8,128)(2,1)}), bf16[8,128,2048]{1,0,2:T(8,128)(2,1)}, u32[]{:S(2)}, u32[]{:S(2)}) async-start(bf16[8,128,2048]{1,0,2:T(8,128)(2,1)} %copy.65), calls=%async_computation.6 | async-start | bytes 8388608 | tf_op jit(solution)/shard_map/all_to_all | solution.py:67
  433.3 7.5 %copy-start.1 = (bf16[8,4,128,512]{3,2,1,0:T(8,128)(2,1)S(1)}, bf16[8,4,128,512]{3,2,1,0:T(8,128)(2,1)}, u32[]{:S(2)}) copy-start(bf16[8,4,128,512]{3,2,1,0:T(8,128)(2,1)} %copy.67) | copy-start | bytes 12582916
Sparse Core Ops, SparseCore 0:
  70.7 36.2 all-gather.5
  115.4 27.8 all-gather.3
  145.5 28.4 all-gather.7
